TPU v7x, 32 devices: a whole 2x2x4 slice. The times are simulated.
32 devices in a mesh: sp: 16 (over z, y, x), tp: 2 (over core).
Axes of the slice: x: 2, y: 2, z: 4, core: 2. Of those that a mesh axis runs over, the one named last changes fastest.
Arguments:
- tokens: bfloat16 [16384, 2048], P('sp', 'tp'), may hold values from -6 to 6
- norm_gain: float32 [2048], replicated, may hold values from 0.1 to 1.9
- w_query: bfloat16 [2048, 1024], P('sp', 'tp'), may hold values from -0.125 to 0.125
- w_key: bfloat16 [2048, 512], P('sp', 'tp'), may hold values from -0.125 to 0.125
- w_value: bfloat16 [2048, 512], P('sp', 'tp'), may hold values from -0.125 to 0.125
- w_glu_a: bfloat16 [2048, 1024], P('sp', 'tp'), may hold values from -0.125 to 0.125
- w_glu_b: bfloat16 [2048, 1024], P('sp', 'tp'), may hold values from -0.125 to 0.125
- q_gain: float32 [64], replicated, may hold values from 0.8 to 7
- k_gain: float32 [64], replicated, may hold values from 0.8 to 7
- sink_logit: float32 [16], P('tp'), may hold values from 1 to 4
- conv_taps: float32 [31, 1024], P(None, 'tp'), may hold values from -1 to 1
- chan_gain: float32 [1024], P('tp'), may hold values from 0.1 to 1.9
- chan_bias: float32 [1024], P('tp'), may hold values from -3 to 3
- w_attn_back: bfloat16 [2048, 1024], P('sp', 'tp'), may hold values from -0.1875 to 0.1875
- w_conv_back: bfloat16 [2048, 1024], P('sp', 'tp'), may hold values from -0.1875 to 0.1875
Outputs:
- mixed: bfloat16 [16384, 2048], P(('sp', 'tp'))
- log_weight: float32 [16, 16384], P('tp', 'sp')
All inputs are finite; a program needn't handle non-finite values.
Results may differ from a plain program's by a relative error of at most 0.014.
The roundings to bfloat16 on the way count: a program that leaves them out, or rounds other values in their place, can miss the bound.
Values may be sent and summed in bfloat16 or wider, within the bound.
A program may use at most 128 MiB of HBM per device.

v0:
```python
import jax
import jax.numpy as jnp
from jax import lax
from jax.sharding import PartitionSpec as P

HEAD = 64
CH = 1024
KW = 31
WINDOW = 128


EPS = 1e-06


def passed_along(value, axis, steps):
    count = lax.axis_size(axis)
    leading, last = (max(0, -steps), min(count, count - steps))
    return lax.ppermute(value, axis, [(source, source + steps) for source in range(leading, last)])


def row_norm(inputs, scale_vec):
    squares = jnp.mean(inputs * inputs, axis=-1, keepdims=True)
    return inputs * lax.rsqrt(squares + EPS) * scale_vec


def local(
    tokens,
    norm_gain,
    w_query,
    w_key,
    w_value,
    w_glu_a,
    w_glu_b,
    q_gain,
    k_gain,
    sink_logit,
    conv_taps,
    chan_gain,
    chan_bias,
    w_attn_back,
    w_conv_back,
):
    row_count = tokens.shape[0]
    q_local = w_query.shape[1] // HEAD
    kv_local = w_key.shape[1] // HEAD
    group_size = q_local // kv_local
    kv_width = kv_local * HEAD
    gathered = lax.all_gather(tokens, "tp", axis=1, tiled=True)
    normed = row_norm(gathered.astype(jnp.float32), norm_gain).astype(jnp.bfloat16)
    whole_rows = (
        lax.all_gather(w_query, "sp", axis=0, tiled=True),
        lax.all_gather(w_key, "sp", axis=0, tiled=True),
        lax.all_gather(w_value, "sp", axis=0, tiled=True),
        lax.all_gather(w_glu_a, "sp", axis=0, tiled=True),
        lax.all_gather(w_glu_b, "sp", axis=0, tiled=True),
        lax.all_gather(w_attn_back, "sp", axis=0, tiled=True),
        lax.all_gather(w_conv_back, "sp", axis=0, tiled=True),
    )
    projected = tuple(
        (jnp.dot(normed, weight, preferred_element_type=jnp.float32) for weight in whole_rows[:5])
    )
    attn_back = whole_rows[5]
    conv_back = whole_rows[6]
    query_raw, key_raw, value_raw, glu_a, glu_b = projected
    queries = row_norm(query_raw.reshape(row_count, q_local, HEAD), q_gain).astype(jnp.bfloat16)
    key_rows = (
        row_norm(key_raw.reshape(row_count, kv_local, HEAD), k_gain)
        .astype(jnp.bfloat16)
        .reshape(row_count, kv_width)
    )
    value_rows = value_raw.astype(jnp.bfloat16)
    gated_rows = (glu_a * jax.nn.sigmoid(glu_b)).astype(jnp.bfloat16)
    key_value = jnp.concatenate([key_rows, value_rows], 1)
    key_value_rim = passed_along(key_value[row_count - WINDOW :], "sp", 1)
    gated_rim = passed_along(gated_rows[row_count - (KW - 1) :], "sp", 1)
    block_count = row_count // WINDOW
    extended = jnp.concatenate([key_value_rim, key_value], 0).reshape(
        block_count + 1, WINDOW, 2 * kv_width
    )
    band = jnp.concatenate([extended[:-1], extended[1:]], 1)
    key_band = band[:, :, :kv_width].reshape(block_count, 2 * WINDOW, kv_local, HEAD)
    value_band = band[:, :, kv_width:].reshape(block_count, 2 * WINDOW, kv_local, HEAD)
    grouped = queries.reshape(block_count, WINDOW, kv_local, group_size, HEAD)
    scores = jnp.einsum(
        "nqhgd,nkhd->nhgqk", grouped, key_band, preferred_element_type=jnp.float32
    ) * HEAD ** (-0.5)
    offsets = jnp.arange(WINDOW, dtype=jnp.int32)
    band_offsets = jnp.arange(2 * WINDOW, dtype=jnp.int32)
    distance = WINDOW + offsets[:, None] - band_offsets[None, :]
    allowed = (distance >= 0) & (distance < WINDOW)
    anchor = lax.axis_index("sp") * row_count
    key_position = (
        anchor
        + jnp.arange(block_count, dtype=jnp.int32)[:, None] * WINDOW
        - WINDOW
        + band_offsets[None, :]
    )
    visible = (allowed[None, :, :] & (key_position[:, None, :] >= 0))[:, None, None]
    sink_table = sink_logit.reshape(kv_local, group_size)[None, :, :, None, None]
    masked = jnp.where(visible, scores, -jnp.inf)
    largest = jnp.maximum(jnp.max(masked, axis=-1, keepdims=True), sink_table)
    weights = jnp.where(visible, jnp.exp(scores - largest), 0.0)
    weight_sum = jnp.sum(weights, axis=-1, keepdims=True) + jnp.exp(sink_table - largest)
    log_weight = (largest + jnp.log(weight_sum))[..., 0]
    log_weight = jnp.transpose(log_weight, (1, 2, 0, 3)).reshape(q_local, row_count)
    probabilities = (weights / weight_sum).astype(jnp.bfloat16)
    attended = jnp.einsum(
        "nhgqk,nkhd->nqhgd", probabilities, value_band, preferred_element_type=jnp.float32
    )
    attended = attended.astype(jnp.bfloat16).reshape(row_count, q_local * HEAD)
    gate_extended = jnp.concatenate([gated_rim, gated_rows], 0).astype(jnp.float32)
    convolved = jnp.zeros((row_count, gated_rows.shape[1]), jnp.float32)
    for tap_index in range(KW):
        convolved = (
            convolved + conv_taps[tap_index] * gate_extended[tap_index : tap_index + row_count]
        )
    channel_sums = lax.psum(
        (jnp.sum(convolved, axis=1), jnp.sum(convolved * convolved, axis=1)), "tp"
    )
    center = (channel_sums[0] / CH)[:, None]
    spread = (channel_sums[1] / CH)[:, None] - center * center
    conv_rows = jax.nn.silu(
        (convolved - center) * lax.rsqrt(spread + EPS) * chan_gain + chan_bias
    ).astype(jnp.bfloat16)
    contract = (((1,), (1,)), ((), ()))
    result = lax.dot_general(attended, attn_back, contract, preferred_element_type=jnp.float32)
    summed = lax.psum_scatter(
        (
            result
            + lax.dot_general(conv_rows, conv_back, contract, preferred_element_type=jnp.float32)
        ).astype(jnp.bfloat16),
        "tp",
        scatter_dimension=0,
        tiled=True,
    )
    return (summed, log_weight)


def solution(mesh):
    placed = (
        P("sp", "tp"),
        P(),
        P("sp", "tp"),
        P("sp", "tp"),
        P("sp", "tp"),
        P("sp", "tp"),
        P("sp", "tp"),
        P(),
        P(),
        P("tp"),
        P(None, "tp"),
        P("tp"),
        P("tp"),
        P("sp", "tp"),
        P("sp", "tp"),
    )
    return jax.shard_map(
        local,
        mesh=mesh,
        in_specs=placed,
        out_specs=(P(("sp", "tp"), None), P("tp", "sp")),
        check_vma=False,
    )
```

profile of v0, /device:TPU:0, one launch (start us, length us, event | category | flops | bytes accessed | tf_op | source)
XLA Modules:
  0.0 476.1 jit_solution(15516827644429883974)
XLA Ops:
  7.2 0.7 all-gather.9.cloned.1.call-update
  8.0 0.7 all-gather.15.cloned.1.call-update
  8.7 0.7 all-gather.11.cloned.1.call-update
  11.2 0.7 all-gather.17.cloned.1.call-update
  11.9 0.7 all-gather.23.cloned.1.call-update
  14.7 11.3 %all-gather.9.cloned.1.call-done = bf16[1024,2048]{1,0:T(8,128)(2,1)} async-done(((bf16[1024,1024]{1,0:T(8,128)(2,1)}), bf16[1024,2048]{1,0:T(8,128)(2,1)}) %all-gather.9.cloned.1.call-update) | async-done | bytes 4194320 | tf_op jit(solution)/shard_map/all_gather | solution.py:48
  26.0 3.1 fusion
  29.1 61.3 %all-gather.15.cloned.1.call-done = bf16[2048,512]{1,0:T(8,128)(2,1)} async-done(((bf16[128,512]{1,0:T(8,128)(2,1)}), bf16[2048,512]{1,0:T(8,128)(2,1)}) %all-gather.15.cloned.1.call-update) | async-done | bytes 2097168 | tf_op jit(solution)/shard_map/all_gather | solution.py:51
  90.3 6.7 %bitcast_reduce_fusion = (f32[1024,8]{0,1:T(8,128)S(1)}, f32[1024,512]{0,1:T(8,128)}) fusion(bf16[2048,512]{1,0:T(8,128)(2,1)} %all-gather.15.cloned.1.call-done, bf16[1024,2048]{1,0:T(8,128)(2,1)} %all-gather.9.cloned.1.call-done, f32[2048]{0:T(1024)S(1)} %copy-done.28, f32[1024]{0:T(1024)S(1)} %add_rsqrt_fusion.3), kind=kOutput, calls=%fused_computation.75 | convolution fusion | flops 2156912640 | bytes 8433664 | tf_op jit(solution)/shard_map/dot_general | solution.py:60
  97.0 50.0 %all-gather.11.cloned.1.call-done = bf16[2048,256]{1,0:T(8,128)(2,1)} async-done(((bf16[128,256]{1,0:T(8,128)(2,1)}), bf16[2048,256]{1,0:T(8,128)(2,1)}) %all-gather.11.cloned.1.call-update) | async-done | bytes 1048592 | tf_op jit(solution)/shard_map/all_gather | solution.py:52
  147.0 4.0 bitcast_reduce_fusion.1
  151.1 57.8 %all-gather.19.cloned.1.call-done = bf16[2048,512]{1,0:T(8,128)(2,1)} async-done(((bf16[128,512]{1,0:T(8,128)(2,1)}), bf16[2048,512]{1,0:T(8,128)(2,1)}) %all-gather.19.cloned.1.call-update) | async-done | bytes 2097168 | tf_op jit(solution)/shard_map/all_gather | solution.py:54
  208.9 6.6 %fusion.69 = f32[1024,512]{1,0:T(8,128)} fusion(bf16[2048,512]{1,0:T(8,128)(2,1)} %all-gather.19.cloned.1.call-done, bf16[1024,2048]{1,0:T(8,128)(2,1)} %all-gather.9.cloned.1.call-done, f32[2048]{0:T(1024)S(1)} %copy-done.28, f32[1024]{0:T(1024)S(1)} %add_rsqrt_fusion.3), kind=kOutput, calls=%fused_computation.135 | convolution fusion | flops 2155872256 | bytes 8400896 | tf_op jit(solution)/shard_map/dot_general | solution.py:60
  215.5 55.2 %all-gather.21.cloned.1.call-done = bf16[2048,512]{1,0:T(8,128)(2,1)} async-done(((bf16[128,512]{1,0:T(8,128)(2,1)}), bf16[2048,512]{1,0:T(8,128)(2,1)}) %all-gather.21.cloned.1.call-update) | async-done | bytes 2097168 | tf_op jit(solution)/shard_map/all_gather | solution.py:55
  270.7 6.1 %multiply_convert_fusion.1 = bf16[1024,512]{1,0:T(8,128)(2,1)S(1)} fusion(f32[1024,512]{1,0:T(8,128)} %fusion.69, bf16[2048,512]{1,0:T(8,128)(2,1)} %all-gather.21.cloned.1.call-done, bf16[1024,2048]{1,0:T(8,128)(2,1)} %all-gather.9.cloned.1.call-done, f32[2048]{0:T(1024)S(1)} %copy-done.28, f32[1024]{0:T(1024)S(1)} %add_rsqrt_fusion.3), kind=kOutput, calls=%fused_computation.81 | convolution fusion | flops 2158493696 | bytes 9449472 | tf_op jit(solution)/shard_map/dot_general | solution.py:60
  276.8 3.4 collective-permute-start.1
  280.4 46.8 %all-gather.13.cloned.1.call-done = bf16[2048,256]{1,0:T(8,128)(2,1)} async-done(((bf16[128,256]{1,0:T(8,128)(2,1)}), bf16[2048,256]{1,0:T(8,128)(2,1)}) %all-gather.13.cloned.1.call-update) | async-done | bytes 1048592 | tf_op jit(solution)/shard_map/all_gather | solution.py:53
  327.2 4.2 convolution_convert_fusion
  331.4 0.7 fusion.58
  332.8 4.0 collective-permute-start
  337.3 9.5 %fusion.76 = (f32[1024]{0:T(1024)S(1)}, f32[1024]{0:T(1024)S(1)}, f32[1024,512]{1,0:T(8,128)}) fusion(f32[1054,512]{1,0:T(8,128)S(1)} %maximum_convert_fusion, f32[512]{0:T(512)S(1)} %bitcast.141, f32[512]{0:T(512)S(1)} %bitcast.142, f32[512]{0:T(512)S(1)} %bitcast.144, f32[512]{0:T(512)S(1)} %bitcast.145, f32[512]{0:T(512)S(1)} %bitcast.146, ...), kind=kLoop, calls=%fused_computation.138 | loop fusion | flops 33552384 | bytes 67180544 | tf_op jit(solution)/shard_map/reduce_sum | solution.py:118
  346.8 2.5 all-reduce
  349.3 1.3 fusion.42
  352.3 1.9 fusion.3
  354.3 2.2 fusion.6
  356.7 2.4 fusion.41
  359.1 0.7 copy.46
  359.8 29.5 %all-gather.17.cloned.1.call-done = bf16[2048,512]{1,0:T(8,128)(2,1)} async-done(((bf16[128,512]{1,0:T(8,128)(2,1)}), bf16[2048,512]{1,0:T(8,128)(2,1)}) %all-gather.17.cloned.1.call-update) | async-done | bytes 2097168 | tf_op jit(solution)/shard_map/all_gather | solution.py:56
  389.3 7.4 %fusion.45 = f32[1024,2048]{1,0:T(8,128)} fusion(bf16[2048,512]{1,0:T(8,128)(2,1)} %all-gather.17.cloned.1.call-done, bf16[64,8,8,128]{3,2,1,0:T(8,128)(2,1)S(1)} %bitcast.127), kind=kOutput, calls=%fused_computation.91 | convolution fusion | flops 2147483648 | bytes 11534336 | tf_op jit(solution)/shard_map/dot_general | solution.py:126
  396.7 54.6 %all-gather.23.cloned.1.call-done = bf16[2048,512]{1,0:T(8,128)(2,1)} async-done(((bf16[128,512]{1,0:T(8,128)(2,1)}), bf16[2048,512]{1,0:T(8,128)(2,1)}) %all-gather.23.cloned.1.call-update) | async-done | bytes 2097168 | tf_op jit(solution)/shard_map/all_gather | solution.py:57
  451.2 7.3 %add_convert_fusion = bf16[1024,2048]{1,0:T(8,128)(2,1)} fusion(f32[1024,2048]{1,0:T(8,128)} %fusion.45, bf16[2048,512]{1,0:T(8,128)(2,1)} %all-gather.23.cloned.1.call-done, f32[1024,512]{1,0:T(8,128)S(1)} %copy-done, f32[512]{0:T(512)S(1)} %copy-done.29, f32[512]{0:T(512)S(1)} %copy-done.30, f32[1024]{0:T(1024)S(1)} %get-tuple-element.43, ...), kind=kOutput, calls=%fused_computation.10 | convolution fusion | flops 2156396544 | bytes 16789504 | tf_op jit(solution)/shard_map/dot_general | solution.py:130
  459.3 10.3 %reduce-scatter.2.cloned.1.call-done = bf16[512,2048]{1,0:T(8,128)(2,1)} async-done(((bf16[1024,2048]{1,0:T(8,128)(2,1)}), bf16[512,2048]{1,0:T(8,128)(2,1)}) %reduce-scatter.2.cloned.1.call-update) | async-done | bytes 2097168 | tf_op jit(solution)/shard_map/reduce_scatter | solution.py:127
  (108 shorter events, 7.7 us)
Async XLA Ops:
  7.2 5.6 %copy-start.4 = (f32[31,512]{1,0:T(8,128)S(1)}, f32[31,512]{1,0:T(8,128)}, u32[]{:S(2)}) copy-start(f32[31,512]{1,0:T(8,128)} %param.25) | copy-start | bytes 190468
  7.2 6.9 %copy-start.26 = (f32[8]{0:T(128)S(1)}, f32[8]{0:T(128)}, u32[]{:S(2)}) copy-start(f32[8]{0:T(128)} %param.24) | copy-start | bytes 100
  7.2 7.0 %copy-start.27 = (f32[64]{0:T(128)S(1)}, f32[64]{0:T(128)}, u32[]{:S(2)}) copy-start(f32[64]{0:T(128)} %param.23) | copy-start | bytes 772
  7.2 18.8 %all-gather.9.cloned.1.call-start = ((), (), s32[]{:S(2)}) async-start(), calls=%async_computation.1 | async-start | bytes 6291456 | tf_op jit(solution)/shard_map/all_gather | solution.py:48
  7.9 82.4 %all-gather.15.cloned.1.call-start = ((), (), s32[]{:S(2)}) async-start(), calls=%async_computation.4 | async-start | bytes 2228224 | tf_op jit(solution)/shard_map/all_gather | solution.py:51
  8.7 138.3 %all-gather.11.cloned.1.call-start = ((), (), s32[]{:S(2)}) async-start(), calls=%async_computation.2 | async-start | bytes 1114112 | tf_op jit(solution)/shard_map/all_gather | solution.py:52
  9.4 199.5 %all-gather.19.cloned.1.call-start = ((), (), s32[]{:S(2)}) async-start(), calls=%async_computation.6 | async-start | bytes 2228224 | tf_op jit(solution)/shard_map/all_gather | solution.py:54
  10.0 260.7 %all-gather.21.cloned.1.call-start = ((), (), s32[]{:S(2)}) async-start(), calls=%async_computation.7 | async-start | bytes 2228224 | tf_op jit(solution)/shard_map/all_gather | solution.py:55
  10.6 316.7 %all-gather.13.cloned.1.call-start = ((), (), s32[]{:S(2)}) async-start(), calls=%async_computation.3 | async-start | bytes 1114112 | tf_op jit(solution)/shard_map/all_gather | solution.py:53
  11.2 378.1 %all-gather.17.cloned.1.call-start = ((), (), s32[]{:S(2)}) async-start(), calls=%async_computation.5 | async-start | bytes 2228224 | tf_op jit(solution)/shard_map/all_gather | solution.py:56
  11.9 439.3 %all-gather.23.cloned.1.call-start = ((), (), s32[]{:S(2)}) async-start(), calls=%async_computation.8 | async-start | bytes 2228224 | tf_op jit(solution)/shard_map/all_gather | solution.py:57
  12.7 457.0 %reduce-scatter.2.cloned.1.call-start = ((), (), s32[]{:S(2)}) async-start(), calls=%async_computation.9 | async-start | bytes 6291456 | tf_op jit(solution)/shard_map/reduce_scatter | solution.py:127
  14.6 75.7 %copy-start.28 = (f32[2048]{0:T(1024)S(1)}, f32[2048]{0:T(1024)}, u32[]{:S(2)}) copy-start(f32[2048]{0:T(1024)} %param.16) | copy-start | bytes 24580
  276.8 59.9 %collective-permute-start.1 = (bf16[30,512]{1,0:T(8,128)(2,1)S(1)}, bf16[30,512]{1,0:T(8,128)(2,1)S(1)}, u32[]{:S(2)}, u32[]{:S(2)}) collective-permute-start(bf16[30,512]{1,0:T(8,128)(2,1)S(1)} %slice.281), channel_id=1, source_target_pairs={{0,2},{2,4},{4,6},{6,8},{8,10},{10,12},{12,14},{14,16},{16,18},{18... | collective-permute-start | bytes 92168 | tf_op jit(solution)/shard_map/ppermute | solution.py:18
  327.2 4.9 %copy-start.1 = (f32[1024,512]{0,1:T(8,128)S(1)}, f32[1024,512]{0,1:T(8,128)}, u32[]{:S(2)}) copy-start(f32[1024,512]{0,1:T(8,128)} %get-tuple-element.47) | copy-start | bytes 6291460
  332.1 4.7 copy-start.3
  332.6 4.6 copy-start.5
  332.6 4.6 copy-start.6
  332.6 4.6 copy-start.7
  332.6 4.6 copy-start.8
  332.6 4.6 copy-start.9
  332.6 4.6 copy-start.10
  332.6 4.6 copy-start.11
  332.6 4.6 copy-start.12
  332.7 4.6 copy-start.13
  332.7 4.6 copy-start.14
  332.7 4.6 copy-start.15
  332.7 4.6 copy-start.16
  332.8 16.5 %collective-permute-start = (bf16[128,512]{0,1:T(8,128)(2,1)}, bf16[128,512]{0,1:T(8,128)(2,1)}, u32[]{:S(2)}, u32[]{:S(2)}) collective-permute-start(bf16[128,512]{0,1:T(8,128)(2,1)} %fusion.58), channel_id=1, source_target_pairs={{0,2},{2,4},{4,6},{6,8},{8,10},{10,12},{12,14},{14,16},{16,18},{18... | collective-permute-start | bytes 393224 | tf_op jit(solution)/shard_map/ppermute | solution.py:18
  389.3 62.0 %copy-start = (f32[1024,512]{1,0:T(8,128)S(1)}, f32[1024,512]{1,0:T(8,128)}, u32[]{:S(2)}) copy-start(f32[1024,512]{1,0:T(8,128)} %get-tuple-element.6) | copy-start | bytes 6291460
  389.3 62.0 %copy-start.29 = (f32[512]{0:T(512)S(1)}, f32[512]{0:T(512)}, u32[]{:S(2)}) copy-start(f32[512]{0:T(512)} %param.27) | copy-start | bytes 6148
  389.3 62.0 %copy-start.30 = (f32[512]{0:T(512)S(1)}, f32[512]{0:T(512)}, u32[]{:S(2)}) copy-start(f32[512]{0:T(512)} %param.26) | copy-start | bytes 6148
  (10 other events, 40.5 us)
Sparse Core Ops, SparseCore 0:
  9.5 16.3 all-gather.8
  28.7 61.5 all-gather.14
  93.1 53.8 all-gather.10
  149.6 59.2 all-gather.18
  211.5 59.1 all-gather.20
  273.3 53.8 all-gather.12
  330.0 59.2 all-gather.16
  392.0 59.1 all-gather.22
  458.7 10.8 reduce-scatter.1
where the time goes:
time: 476 us
  waiting for transfers between devices  382 us (80%)
  matrix products  46.7 us (10%)
  other arithmetic  18 us (4%)
  between operations  14.4 us (3%)
  starting transfers between devices  7.71 us (2%)
  local copies, waits for them, and re-layouts  5.14 us (1%)
    all_gather x1, waiting for transfers between devices, local(): lax.all_gather(w_query, 'sp', axis=0, tiled=True)  61.3 us
    all_gather x1, waiting for transfers between devices, local(): lax.all_gather(w_glu_a, 'sp', axis=0, tiled=True)  57.8 us
    all_gather x1, waiting for transfers between devices, local(): lax.all_gather(w_glu_b, 'sp', axis=0, tiled=True)  55.2 us
    all_gather x1, waiting for transfers between devices, local(): lax.all_gather(w_conv_back, 'sp', axis=0, tiled=True)  54.6 us
    all_gather x1, waiting for transfers between devices, local(): lax.all_gather(w_key, 'sp', axis=0, tiled=True)  50 us
    all_gather x1, waiting for transfers between devices, local(): lax.all_gather(w_value, 'sp', axis=0, tiled=True)  46.8 us
    all_gather x1, waiting for transfers between devices, local(): lax.all_gather(w_attn_back, 'sp', axis=0, tiled=True)  29.5 us
    dot_general x5, matrix products, local(): jnp.dot(normed, weight, preferred_element_type=jnp.float32)  27.6 us
  transfers between devices with their start and end apart: 11, of which 9 were waited for; matrix products, arithmetic and copies ran while one was open for 13% of the time, Pallas kernels for 0%

commit v1 on v0

--- a/solution.py
+++ b/solution.py
@@ -1,6 +1,11 @@
+import functools
+import itertools
+
 import jax
 import jax.numpy as jnp
 from jax import lax
+from jax.experimental import pallas as pl
+from jax.experimental.pallas import tpu as pltpu
 from jax.sharding import PartitionSpec as P
 
 HEAD = 64
@@ -21,6 +26,189 @@
 def row_norm(inputs, scale_vec):
     squares = jnp.mean(inputs * inputs, axis=-1, keepdims=True)
     return inputs * lax.rsqrt(squares + EPS) * scale_vec
+
+
+MESH = pl.DeviceIdType.MESH
+ORDERS = ("xzy", "yzx", "xzy", "yzx", "zxy", "zyx")
+STARTS = (0, 0, 1, 1, 2, 2)
+BLOCK = 256
+
+
+def gather_kernel(
+    n_sp, n_tp, tok, gain, wa, wb, wq, wkv, wo, wc, gated, query, key_value, back,
+    rows_full, fa, fb, fq, fkv, recv, send, tok_recv, tok_send, own_sem,
+):
+    me, core = lax.axis_index("sp"), lax.axis_index("tp")
+    depth = n_sp // 4
+    x, y, z = me % 2, (me // 2) % 2, me // 4
+    near = {
+        "x": (me - x + (1 - x), None),
+        "y": (me - 2 * y + 2 * (1 - y), None),
+        "up": (me + 4, z < depth - 1),
+        "down": (me - 4, z > 0),
+    }
+    lanes = {name: index for index, name in enumerate(near)}
+    shards = (wa, wb, wq, wkv, wo, wc)
+    shard_rows, width = wa.shape
+    wholes = (fa, fb, fq, fkv, back.at[:, pl.ds(0, width)], back.at[:, pl.ds(width, width)])
+
+    def guarded(conditions, action):
+        known = [condition for condition in conditions if condition is not None]
+        if not known:
+            action()
+        else:
+            pl.when(functools.reduce(jnp.logical_and, known))(action)
+
+    barrier = pltpu.get_barrier_semaphore()
+    for name, (target, exists) in near.items():
+        guarded((exists,), lambda target=target: pl.semaphore_signal(
+            barrier, inc=1, device_id=(target, core), device_id_type=MESH))
+    for step in range(1, n_tp):
+        pl.semaphore_signal(
+            barrier, inc=1, device_id=(me, lax.rem(core + step, n_tp)), device_id_type=MESH)
+    ends = jnp.where(z < depth - 1, 1, 0) + jnp.where(z > 0, 1, 0)
+    pl.semaphore_wait(barrier, 2 + (n_tp - 1) + ends)
+
+    tok_width = tok.shape[1]
+
+    def tok_columns(owner):
+        return rows_full.at[:, pl.ds(pl.multiple_of(owner * tok_width, tok_width), tok_width)]
+
+    def tok_copy(step):
+        return pltpu.make_async_remote_copy(
+            src_ref=tok, dst_ref=tok_columns(core),
+            send_sem=tok_send.at[step - 1], recv_sem=tok_recv.at[step - 1],
+            device_id=(me, lax.rem(core + step, n_tp)), device_id_type=MESH)
+
+    def spot(chunk, owner):
+        return wholes[chunk].at[pl.ds(pl.multiple_of(owner * shard_rows, shard_rows), shard_rows), :]
+
+    def block_copy(chunk, owner, name, own):
+        return pltpu.make_async_remote_copy(
+            src_ref=shards[chunk] if own else spot(chunk, owner),
+            dst_ref=spot(chunk, owner),
+            send_sem=send.at[chunk, owner, lanes[name]], recv_sem=recv.at[chunk, owner],
+            device_id=(near[name][0], core), device_id_type=MESH)
+
+    def blocks(chunk):
+        order = ORDERS[chunk]
+        for dx, dy, dz in itertools.product((0, 1), (0, 1), range(1 - depth, depth)):
+            moved = {"x": dx, "y": dy, "z": dz}
+            last = max([order.index(axis) for axis in order if moved[axis]], default=-1)
+            onward = []
+            for place, axis in enumerate(order):
+                if axis == "z":
+                    if place > last or (place == last and dz < 0):
+                        onward.append("up")
+                    if place > last or (place == last and dz > 0):
+                        onward.append("down")
+                elif place > last:
+                    onward.append(axis)
+            owner = (z + dz) * 4 + jnp.where(y == 0, dy, 1 - dy) * 2 + jnp.where(x == 0, dx, 1 - dx)
+            inside = None if dz == 0 else (z + dz >= 0 if dz < 0 else z + dz < depth)
+            yield dx + dy + abs(dz), owner, inside, onward
+
+    plan = [sorted(blocks(chunk), key=lambda item: item[0]) for chunk in range(len(shards))]
+    hops = depth + 1
+
+    def relay(chunk, hop):
+        for distance, owner, inside, onward in plan[chunk]:
+            if distance != hop:
+                continue
+
+            def step(owner=owner, onward=onward):
+                if hop:
+                    block_copy(chunk, owner, "x", False).wait_recv()
+                for name in onward:
+                    guarded((near[name][1],), lambda name=name: block_copy(
+                        chunk, owner, name, hop == 0).start())
+            guarded((inside,), step)
+
+    own_copies = [
+        pltpu.make_async_copy(shards[chunk], spot(chunk, me), own_sem.at[chunk])
+        for chunk in range(len(shards))
+    ] + [pltpu.make_async_copy(tok, tok_columns(core), own_sem.at[len(shards)])]
+
+    row_blocks = tok.shape[0] // BLOCK
+
+    def row_slice(index):
+        return pl.ds(pl.multiple_of(index * BLOCK, BLOCK), BLOCK)
+
+    def normalise():
+        for step in range(1, n_tp):
+            tok_copy(step).wait_recv()
+
+        @pl.loop(0, tok.shape[0] // 64)
+        def _(index):
+            rows = pl.ds(pl.multiple_of(index * 64, 64), 64)
+            rows_full[rows, :] = row_norm(
+                rows_full[rows, :].astype(jnp.float32), gain[...]).astype(jnp.bfloat16)
+
+    def project(weights):
+        def dot(rows, weight):
+            return jnp.dot(rows_full[rows, :], weight[...], preferred_element_type=jnp.float32)
+
+        @pl.loop(0, row_blocks)
+        def _(index):
+            rows = row_slice(index)
+            if weights == "gate":
+                gated[rows, :] = (dot(rows, fa) * jax.nn.sigmoid(dot(rows, fb))).astype(jnp.bfloat16)
+            elif weights == "query":
+                query[rows, :] = dot(rows, fq)
+            else:
+                key_value[rows, :] = dot(rows, fkv)
+
+    after = {1: "gate", 2: "query", 3: "key_value"}
+    for tick in range(max(STARTS) + hops + 1):
+        for chunk, start in enumerate(STARTS):
+            if 0 <= tick - start <= hops:
+                relay(chunk, tick - start)
+        if tick == 0:
+            for step in range(1, n_tp):
+                tok_copy(step).start()
+            for copy in own_copies:
+                copy.start()
+            for copy in own_copies:
+                copy.wait()
+            normalise()
+        for chunk, start in enumerate(STARTS):
+            if tick - start == hops and chunk in after:
+                project(after[chunk])
+    for step in range(1, n_tp):
+        tok_copy(step).wait_send()
+    for chunk in range(len(shards)):
+        for distance, owner, inside, onward in plan[chunk]:
+            for name in onward:
+                guarded((inside, near[name][1]), lambda chunk=chunk, owner=owner, name=name,
+                        own=distance == 0: block_copy(chunk, owner, name, own).wait_send())
+
+
+def gather_and_project(tokens, norm_gain, wa, wb, wq, wkv, wo, wc):
+    n_sp, n_tp = lax.axis_size("sp"), lax.axis_size("tp")
+    rows, features = tokens.shape[0], tokens.shape[1] * n_tp
+    model, width = wa.shape[0] * n_sp, wa.shape[1]
+    vmem = pl.BlockSpec(memory_space=pltpu.VMEM)
+    return pl.pallas_call(
+        functools.partial(gather_kernel, n_sp, n_tp),
+        out_shape=(
+            jax.ShapeDtypeStruct((rows, width), jnp.bfloat16),
+            jax.ShapeDtypeStruct((rows, width), jnp.float32),
+            jax.ShapeDtypeStruct((rows, wkv.shape[1]), jnp.float32),
+            jax.ShapeDtypeStruct((model, 2 * width), jnp.bfloat16),
+        ),
+        in_specs=[vmem] * 8,
+        out_specs=(vmem, vmem, vmem, pl.BlockSpec(memory_space=pl.ANY)),
+        scratch_shapes=[pltpu.VMEM((rows, features), jnp.bfloat16)]
+        + [pltpu.VMEM((model, width), jnp.bfloat16)] * 4
+        + [
+            pltpu.SemaphoreType.DMA((6, n_sp)),
+            pltpu.SemaphoreType.DMA((6, n_sp, 4)),
+            pltpu.SemaphoreType.DMA((n_tp - 1,)),
+            pltpu.SemaphoreType.DMA((n_tp - 1,)),
+            pltpu.SemaphoreType.DMA((7,)),
+        ],
+        compiler_params=pltpu.CompilerParams(collective_id=0, has_side_effects=True),
+    )(tokens, norm_gain.reshape(1, features), wa, wb, wq, wkv, wo, wc)
 
 
 def local(
@@ -45,23 +233,11 @@
     kv_local = w_key.shape[1] // HEAD
     group_size = q_local // kv_local
     kv_width = kv_local * HEAD
-    gathered = lax.all_gather(tokens, "tp", axis=1, tiled=True)
-    normed = row_norm(gathered.astype(jnp.float32), norm_gain).astype(jnp.bfloat16)
-    whole_rows = (
-        lax.all_gather(w_query, "sp", axis=0, tiled=True),
-        lax.all_gather(w_key, "sp", axis=0, tiled=True),
-        lax.all_gather(w_value, "sp", axis=0, tiled=True),
-        lax.all_gather(w_glu_a, "sp", axis=0, tiled=True),
-        lax.all_gather(w_glu_b, "sp", axis=0, tiled=True),
-        lax.all_gather(w_attn_back, "sp", axis=0, tiled=True),
-        lax.all_gather(w_conv_back, "sp", axis=0, tiled=True),
-    )
-    projected = tuple(
-        (jnp.dot(normed, weight, preferred_element_type=jnp.float32) for weight in whole_rows[:5])
-    )
-    attn_back = whole_rows[5]
-    conv_back = whole_rows[6]
-    query_raw, key_raw, value_raw, glu_a, glu_b = projected
+    gated_rows, query_raw, key_value_raw, back = gather_and_project(
+        tokens, norm_gain, w_glu_a, w_glu_b, w_query,
+        jnp.concatenate([w_key, w_value], 1), w_attn_back, w_conv_back,
+    )
+    key_raw, value_raw = key_value_raw[:, :kv_width], key_value_raw[:, kv_width:]
     queries = row_norm(query_raw.reshape(row_count, q_local, HEAD), q_gain).astype(jnp.bfloat16)
     key_rows = (
         row_norm(key_raw.reshape(row_count, kv_local, HEAD), k_gain)
@@ -69,7 +245,6 @@
         .reshape(row_count, kv_width)
     )
     value_rows = value_raw.astype(jnp.bfloat16)
-    gated_rows = (glu_a * jax.nn.sigmoid(glu_b)).astype(jnp.bfloat16)
     key_value = jnp.concatenate([key_rows, value_rows], 1)
     key_value_rim = passed_along(key_value[row_count - WINDOW :], "sp", 1)
     gated_rim = passed_along(gated_rows[row_count - (KW - 1) :], "sp", 1)
@@ -122,17 +297,24 @@
     conv_rows = jax.nn.silu(
         (convolved - center) * lax.rsqrt(spread + EPS) * chan_gain + chan_bias
     ).astype(jnp.bfloat16)
+    both = jnp.concatenate([attended, conv_rows], 1)
     contract = (((1,), (1,)), ((), ()))
-    result = lax.dot_general(attended, attn_back, contract, preferred_element_type=jnp.float32)
-    summed = lax.psum_scatter(
-        (
-            result
-            + lax.dot_general(conv_rows, conv_back, contract, preferred_element_type=jnp.float32)
-        ).astype(jnp.bfloat16),
-        "tp",
-        scatter_dimension=0,
-        tiled=True,
-    )
+
+    def mixed(rows):
+        return lax.dot_general(rows, back, contract, preferred_element_type=jnp.float32).astype(
+            jnp.bfloat16
+        )
+
+    n_tp = lax.axis_size("tp")
+    if n_tp == 2:
+        half = row_count // 2
+        core = lax.axis_index("tp")
+        theirs = mixed(lax.dynamic_slice_in_dim(both, (1 - core) * half, half, 0))
+        arrived = lax.ppermute(theirs, "tp", [(0, 1), (1, 0)])
+        ours = mixed(lax.dynamic_slice_in_dim(both, core * half, half, 0))
+        summed = (ours.astype(jnp.float32) + arrived.astype(jnp.float32)).astype(jnp.bfloat16)
+    else:
+        summed = lax.psum_scatter(mixed(both), "tp", scatter_dimension=0, tiled=True)
     return (summed, log_weight)
 
 

time: 476 us -> 193 us (0.41)
  waiting for transfers between devices: 382 us -> 3.61 us
  Pallas kernels: 0 us -> 114 us
  matrix products: 46.7 us -> 16.7 us
  between operations: 14.4 us -> 1.09 us
  local copies, waits for them, and re-layouts: 5.14 us -> 18.4 us
  other arithmetic: 18 us -> 28.6 us
    all_gather x8 -> x0, waiting for transfers between devices: 366 us -> none  [the longest x1 61.3 us: local(): lax.all_gather(w_query, 'sp', axis=0, tiled=True)]
    pallas_call x0 -> x1, Pallas kernels: none -> 114 us  [gather_and_project(): pl.pallas_call(functools.partial(gather_kernel, n_sp, n_tp), out_shape=(j...]
    dot_general x7 -> x2, matrix products: 42.4 us -> 12.7 us  [mixed(): lax.dot_general(rows, back, contract, preferred_element_type=jnp.float32)]
    reduce_scatter x1 -> x0, waiting for transfers between devices: 10.3 us -> none  [local(): lax.psum_scatter((result + lax.dot_general(conv_rows, conv_back, contract...]
    unnamed x9 -> x0, waiting for transfers between devices: 5.04 us -> none
  transfers between devices with their start and end apart: 11 -> 3, of which waited for: 9 -> 1; matrix products, arithmetic and copies ran while one was open for 13% -> 16% of each run, Pallas kernels for 0% -> 0%
where the time goes in v1:
time: 193 us
  Pallas kernels  114 us (59%)
  other arithmetic  28.6 us (15%)
  local copies, waits for them, and re-layouts  18.4 us (10%)
  matrix products  16.7 us (9%)
  starting transfers between devices  7.25 us (4%)
  waiting for transfers between devices  3.61 us (2%)
  blocking collectives  3.09 us (2%)
    pallas_call x1, Pallas kernels, gather_and_project(): pl.pallas_call(functools.partial(gather_kernel, n_sp, n_tp), out_shape=(j...  114 us
    dot_general x2, matrix products, mixed(): lax.dot_general(rows, back, contract, preferred_element_type=jnp.float32)  12.7 us
    reduce_sum x1, other arithmetic, local(): jnp.sum(convolved, axis=1)  9.91 us
    ppermute x2, starting transfers between devices, passed_along(): lax.ppermute(value, axis, [(source, source + steps) for source in range(l...  7.08 us
    unnamed x51, local copies, waits for them, and re-layouts  4.28 us
  transfers between devices with their start and end apart: 3, of which 1 were waited for; matrix products, arithmetic and copies ran while one was open for 16% of the time, Pallas kernels for 0%

profile of v1, /device:TPU:0, one launch (start us, length us, event | category | flops | bytes accessed | tf_op | source)
XLA Modules:
  0.0 192.8 jit_solution(11662309938148894993)
XLA Ops:
  0.6 1.5 pad_maximum_fusion.4.wkv
  2.2 114.1 %shard_map.158 = (bf16[1024,512]{1,0:T(8,128)(2,1)}, f32[1024,512]{1,0:T(8,128)}, f32[1024,512]{1,0:T(8,128)}, bf16[2048,1024]{1,0:T(8,128)(2,1)}) custom-call(bf16[1024,1024]{1,0:T(8,128)(2,1)} %tok.1, f32[1,2048]{1,0:T(1,128)} %bitcast.112, bf16[128,512]{1,0:T(8,128)(2,1)} %wa.1, bf16[128,512]{1,0:T(8,128)(2,1)} %wb.1, bf16[128,512]{1,0:T(8,128)(2,1)} %wq.1, ...), custom_call_target="tpu_custom_call" | custom-call | tf_op jit(solution)/shard_map/pallas_call | solution.py:191
  116.2 1.3 slice.488
  117.5 1.3 slice_multiply_fusion.31
  119.4 1.3 copy.47
  120.8 1.8 multiply_convert_fusion.2
  122.6 0.7 fusion.44
  123.3 3.4 %collective-permute-start = (bf16[128,512]{1,0:T(8,128)(2,1)}, bf16[128,512]{1,0:T(8,128)(2,1)S(1)}, u32[]{:S(2)}, u32[]{:S(2)}) collective-permute-start(bf16[128,512]{1,0:T(8,128)(2,1)} %fusion.44), channel_id=1, source_target_pairs={{0,2},{2,4},{4,6},{6,8},{8,10},{10,12},{12,14},{14,16},{16,18},{18... | collective-permute-start | bytes 393224 | tf_op jit(solution)/shard_map/ppermute | solution.py:23
  126.7 1.4 slice.224
  128.1 3.7 %collective-permute-start.1 = (bf16[30,512]{1,0:T(8,128)(2,1)}, bf16[30,512]{1,0:T(8,128)(2,1)}, u32[]{:S(2)}, u32[]{:S(2)}) collective-permute-start(bf16[30,512]{1,0:T(8,128)(2,1)} %slice.224), channel_id=1, source_target_pairs={{0,2},{2,4},{4,6},{6,8},{8,10},{10,12},{12,14},{14,16},{16,18},{18... | collective-permute-start | bytes 92168 | tf_op jit(solution)/shard_map/ppermute | solution.py:23
  131.8 1.8 copy.50
  133.6 1.8 mul.428
  135.5 0.7 fusion.47
  136.1 3.5 %copy.66 = f32[64,8,8,128]{3,2,1,0:T(8,128)} copy(f32[64,8,8,128]{3,1,2,0:T(8,128)} %bitcast.103) | data formatting | bytes 4194304
  139.7 1.8 copy.51
  141.5 2.0 %bitcast_reduce_fusion = f32[1024,8]{0,1:T(8,128)S(1)} fusion(f32[1024,512]{0,1:T(8,128)} %copy.51), kind=kLoop, calls=%fused_computation.78 | loop fusion | flops 516096 | bytes 2129920 | tf_op jit(solution)/shard_map/reduce_sum | solution.py:27
  143.5 0.7 fusion.59
  144.6 1.3 multiply_convert_fusion.1
  146.7 1.1 maximum_convert_fusion
  147.9 9.9 %fusion.57 = (f32[1024]{0:T(1024)S(1)}, f32[1024]{0:T(1024)S(1)}, f32[1024,512]{1,0:T(8,128)S(1)}) fusion(f32[1054,512]{1,0:T(8,128)S(1)} %maximum_convert_fusion, f32[512]{0:T(512)S(1)} %bitcast.142, f32[512]{0:T(512)S(1)} %bitcast.143, f32[512]{0:T(512)} %bitcast.114, f32[512]{0:T(512)} %bitcast.115, f32[512]{0:T(512)} %bitcast.116, f32[512]{0:T(512)} %bitcast.117, ...), kind=kLoop, calls=%fused_computation.128 | loop fusion | flops 33552384 | bytes 67180544 | tf_op jit(solution)/shard_map/reduce_sum | solution.py:293
  157.8 3.1 %all-reduce = (f32[1024]{0:T(1024)S(1)}, f32[1024]{0:T(1024)}) all-reduce(f32[1024]{0:T(1024)S(1)} %get-tuple-element.11, f32[1024]{0:T(1024)S(1)} %get-tuple-element.10), channel_id=1, replica_groups=mesh['sp'=16,'tp'=2] {'tp'}, use_global_device_ids=true, to_apply=%region_7.8 | all-reduce | flops 2048 | bytes 16384 | tf_op jit(solution)/shard_map/psum | solution.py:292
  160.9 0.7 broadcast_multiply_fusion
  161.6 2.5 %multiply_convert_fusion = bf16[1024,512]{1,0:T(8,128)(2,1)} fusion(f32[1024,512]{1,0:T(8,128)S(1)} %get-tuple-element.14, f32[512]{0:T(512)} %param.27, f32[512]{0:T(512)} %param.26, f32[1024]{0:T(1024)S(1)} %get-tuple-element.51, f32[1024]{0:T(1024)S(1)} %get-tuple-element.50), kind=kLoop, calls=%fused_computation.79 | loop fusion | flops 4718592 | bytes 3158016 | tf_op jit(solution)/shard_map/convert_element_type | solution.py:299
  164.4 1.3 copy.48
  166.3 1.6 fusion
  168.0 2.2 %fusion.3 = f32[8,4,2,128]{3,2,1,0:T(2,128)S(1)} fusion(f32[8,4,256,128,2]{3,2,4,1,0:T(8,128)S(1)} %get-tuple-element.53, f32[8,4,2,128]{3,2,1,0:T(2,128)S(1)} %copy.54, pred[8,128,256]{1,2,0:T(8,128)(4,1)S(1)} %broadcast_and_fusion), kind=kLoop, calls=%fused_computation.6 | loop fusion | flops 8380416 | bytes 8716288 | tf_op jit(solution)/shard_map/reduce_sum | solution.py:278
  170.4 2.4 %fusion.36 = bf16[8,128,4,2,64]{1,4,3,2,0:T(8,128)(2,1)S(1)} fusion(bf16[8,256,4,64,1]{1,3,4,2,0:T(8,128)(2,1)S(1)} %bitcast.108, f32[8,4,256,128,2]{3,2,4,1,0:T(8,128)S(1)} %get-tuple-element.53, f32[8,4,2,128]{3,2,1,0:T(2,128)S(1)} %copy.56, f32[8,4,2,128]{3,2,1,0:T(2,128)S(1)} %copy.54, pred[8,128,256]{1,2,0:T(8,128)(4,1)S(1)} %broadcast_and_fusion), kind=kOutput, calls=%fused_computation.83 | convolution fusion | flops 279445504 | bytes 10813440 | tf_op jit(solution)/shard_map/nhgqk,nkhd->nqhgd/dot_general | solution.py:282
  172.8 1.5 copy.64
  174.3 1.3 reshape.152
  175.6 6.1 %convolution_convert_fusion = bf16[512,2048]{1,0:T(8,128)(2,1)} fusion(bf16[2048,1024]{1,0:T(8,128)(2,1)} %get-tuple-element.9, s32[]{:T(128)S(6)} %select_n.16, bf16[1024,512]{1,0:T(8,128)(2,1)S(1)} %reshape.152, bf16[1024,512]{1,0:T(8,128)(2,1)} %multiply_convert_fusion), kind=kOutput, calls=%fused_computation.9 | convolution fusion | flops 2150629376 | bytes 8388612 | tf_op jit(solution)/shard_map/dot_general | solution.py:304
  182.6 3.6 %collective-permute-done.2 = bf16[512,2048]{1,0:T(8,128)(2,1)} collective-permute-done((bf16[512,2048]{1,0:T(8,128)(2,1)}, bf16[512,2048]{1,0:T(8,128)(2,1)}, u32[]{:S(2)}, u32[]{:S(2)}) %collective-permute-start.2) | collective-permute-done | bytes 2097184 | tf_op jit(solution)/shard_map/ppermute | solution.py:313
  186.2 6.6 %add_convert_fusion = bf16[512,2048]{1,0:T(8,128)(2,1)} fusion(bf16[512,2048]{1,0:T(8,128)(2,1)} %collective-permute-done.2, bf16[2048,1024]{1,0:T(8,128)(2,1)} %get-tuple-element.9, s32[]{:T(128)S(6)} %select_n.15, bf16[1024,512]{1,0:T(8,128)(2,1)S(1)} %reshape.152, bf16[1024,512]{1,0:T(8,128)(2,1)S(1)} %copy-done.5), kind=kOutput, calls=%fused_computation.7 | convolution fusion | flops 2154823680 | bytes 10485764 | tf_op jit(solution)/shard_map/dot_general | solution.py:304
  (74 shorter events, 3.9 us)
Async XLA Ops:
  119.2 1.6 copy-start.21
  120.7 11.0 %copy-start = (f32[1024,512]{1,0:T(8,128)S(1)}, f32[1024,512]{1,0:T(8,128)}, u32[]{:S(2)}) copy-start(f32[1024,512]{1,0:T(8,128)} %get-tuple-element.7) | copy-start | bytes 6291460
  123.3 40.8 %collective-permute-start = (bf16[128,512]{1,0:T(8,128)(2,1)}, bf16[128,512]{1,0:T(8,128)(2,1)S(1)}, u32[]{:S(2)}, u32[]{:S(2)}) collective-permute-start(bf16[128,512]{1,0:T(8,128)(2,1)} %fusion.44), channel_id=1, source_target_pairs={{0,2},{2,4},{4,6},{6,8},{8,10},{10,12},{12,14},{14,16},{16,18},{18... | collective-permute-start | bytes 393224 | tf_op jit(solution)/shard_map/ppermute | solution.py:23
  128.1 18.6 %collective-permute-start.1 = (bf16[30,512]{1,0:T(8,128)(2,1)}, bf16[30,512]{1,0:T(8,128)(2,1)}, u32[]{:S(2)}, u32[]{:S(2)}) collective-permute-start(bf16[30,512]{1,0:T(8,128)(2,1)} %slice.224), channel_id=1, source_target_pairs={{0,2},{2,4},{4,6},{6,8},{8,10},{10,12},{12,14},{14,16},{16,18},{18... | collective-permute-start | bytes 92168 | tf_op jit(solution)/shard_map/ppermute | solution.py:23
  136.1 3.6 %copy-start.1 = (f32[1024,512]{1,0:T(8,128)S(1)}, f32[1024,512]{1,0:T(8,128)}, u32[]{:S(2)}) copy-start(f32[1024,512]{1,0:T(8,128)} %mul.428) | copy-start | bytes 6291460
  141.5 2.1 %copy-start.8 = (f32[31,512]{1,0:T(8,128)S(1)}, f32[31,512]{1,0:T(8,128)}, u32[]{:S(2)}) copy-start(f32[31,512]{1,0:T(8,128)} %param.25) | copy-start | bytes 190468
  141.5 2.7 %copy-start.7 = (pred[128,256]{0,1:T(8,128)(4,1)S(1)}, pred[128,256]{0,1:T(8,128)(4,1)}, u32[]{:S(2)}) copy-start(pred[128,256]{0,1:T(8,128)(4,1)} %fusion.47) | copy-start | bytes 98308
  141.5 3.1 %copy-start.2 = (f32[64,8,8,128]{3,2,1,0:T(8,128)S(1)}, f32[64,8,8,128]{3,2,1,0:T(8,128)}, u32[]{:S(2)}) copy-start(f32[64,8,8,128]{3,2,1,0:T(8,128)} %copy.66) | copy-start | bytes 6291460
  141.5 3.1 %copy-start.23 = (f32[64]{0:T(128)S(1)}, f32[64]{0:T(128)}, u32[]{:S(2)}) copy-start(f32[64]{0:T(128)} %param.22) | copy-start | bytes 772
  143.5 3.0 %copy-start.22 = (f32[8]{0:T(128)S(1)}, f32[8]{0:T(128)}, u32[]{:S(2)}) copy-start(f32[8]{0:T(128)} %param.24) | copy-start | bytes 100
  143.5 3.2 %copy-start.4 = (bf16[1024,512]{1,0:T(8,128)(2,1)S(1)}, bf16[1024,512]{1,0:T(8,128)(2,1)}, u32[]{:S(2)}) copy-start(bf16[1024,512]{1,0:T(8,128)(2,1)} %get-tuple-element.8) | copy-start | bytes 3145732
  146.6 1.2 copy-start.9
  146.6 1.2 copy-start.10
  146.6 1.2 copy-start.11
  146.6 1.2 copy-start.12
  146.6 1.2 copy-start.13
  146.6 1.2 copy-start.14
  146.6 1.2 copy-start.15
  146.6 1.2 copy-start.16
  146.6 1.2 copy-start.17
  146.6 1.2 copy-start.18
  146.6 1.2 copy-start.19
  146.6 1.2 copy-start.20
  164.4 1.8 copy-start.3
  168.0 2.4 %copy-start.6 = (bf16[8,256,256]{1,2,0:T(8,128)(2,1)S(1)}, bf16[8,256,256]{1,2,0:T(8,128)(2,1)}, u32[]{:S(2)}) copy-start(bf16[8,256,256]{1,2,0:T(8,128)(2,1)} %copy.48) | copy-start | bytes 3145732
  175.6 10.6 %copy-start.5 = (bf16[1024,512]{1,0:T(8,128)(2,1)S(1)}, bf16[1024,512]{1,0:T(8,128)(2,1)}, u32[]{:S(2)}) copy-start(bf16[1024,512]{1,0:T(8,128)(2,1)} %multiply_convert_fusion) | copy-start | bytes 3145732
  181.7 4.5 %collective-permute-start.2 = (bf16[512,2048]{1,0:T(8,128)(2,1)}, bf16[512,2048]{1,0:T(8,128)(2,1)}, u32[]{:S(2)}, u32[]{:S(2)}) collective-permute-start(bf16[512,2048]{1,0:T(8,128)(2,1)} %convolution_convert_fusion), channel_id=1, source_target_pairs={{0,1},{1,0},{2,3},{3,2},{4,5},{5,4},{6,7},{7,6},{8,9},{9,8},{10,11... | collective-permute-start | bytes 6291464 | tf_op jit(solution)/shard_map/ppermute | solution.py:313
